TPU v7x, 32 devices: a whole 2x2x4 slice. The times are simulated.
32 devices in a mesh: ep: 8 (over z, y), tp: 4 (over x, core).
Axes of the slice: x: 2, y: 2, z: 4, core: 2. Of those that a mesh axis runs over, the one named last changes fastest.
Arguments:
- cell_query_rows: bfloat16 [2048, 2048], P('ep', 'tp'), may hold values from -6 to 6
- cell_key_rows: bfloat16 [2048, 2048], P('ep', 'tp'), may hold values from -6 to 6
- cell_value_rows: bfloat16 [2048, 2048], P('ep', 'tp'), may hold values from -6 to 6
- output_gate_logits: bfloat16 [2048, 2048], P('ep', 'tp'), may hold values from -8 to 8
- log_input_gate: float32 [8, 2048], P('tp', 'ep'), may hold values from -4 to 110
- forget_gate_logits: float32 [8, 2048], P('tp', 'ep'), may hold values from -1 to 25
- extra_log_forget: float32 [8, 2048], P('tp', 'ep'), may hold values from -0.7 to 0
- cell_output_scale: float32 [2048], P('tp'), may hold values from 0.1 to 1.9
- tokens_into_experts: bfloat16 [4096, 2048], P(('ep', 'tp')), may hold values from -6 to 6
- expert_norm_scale: float32 [2048], replicated, may hold values from 0.1 to 1.9
- token_expert_index: int32 [4096, 2], P(('ep', 'tp')), may hold values from 0 to 7, all different within a row; in each aligned block of 128 rows (0 to 127, 128 to 255, ...) at most 40 rows name the same one
- chosen_expert_weight: float32 [4096, 2], P(('ep', 'tp')), may hold values from 0.3 to 3
- expert_gate_weight: bfloat16 [8, 2048, 3584], P('ep', None, 'tp'), may hold values from -0.125 to 0.125
- expert_up_weight: bfloat16 [8, 2048, 3584], P('ep', None, 'tp'), may hold values from -0.125 to 0.125
- expert_down_weight: bfloat16 [8, 3584, 2048], P('ep', 'tp'), may hold values from -0.09375 to 0.09375
Outputs:
- gated_head_output: bfloat16 [2048, 2048], P('ep', 'tp')
- expert_output: bfloat16 [4096, 2048], P(('ep', 'tp'))
Inputs may be any that keep to these rules, and one draw needn't show every extreme that they name: `token_expert_index`: each row names 2 different experts. Among the rows of one device (aligned blocks of 128 rows) no expert is named by more than 40 rows, and in every draw some expert is named by exactly 40 rows of some device.
All inputs are finite; a program needn't handle non-finite values.
Results may differ from a plain program's by a relative error of at most 0.012.
Values may be sent and summed in bfloat16 or wider, within the bound.
A program may use at most 128 MiB of HBM per device.

v0:
```python
import jax
import jax.numpy as jnp
from jax import lax
from jax.sharding import PartitionSpec as P

HEAD_DIM = 256
BLOCK = 64
TOPK = 2


EPSILON = 1e-06
PRECISE = lax.Precision.HIGHEST


def carried_in(x, axis, combine, identity):
    size, here = (lax.axis_size(axis), lax.axis_index(axis))
    everything = jax.tree.map(lambda part: lax.all_gather(part, axis), x)
    start = jax.tree.map(
        lambda part, zero: jnp.broadcast_to(jnp.asarray(zero, part.dtype), part.shape), x, identity
    )

    def step(k, before):
        reached = k < here
        new = combine(before, jax.tree.map(lambda part: part[k], everything))
        return jax.tree.map(lambda a, b: jnp.where(reached, a, b), new, before)

    return lax.fori_loop(0, size, step, start)


def combine(earlier, later):
    cell_early, norm_early, stab_early, total_early = earlier
    cell_late, norm_late, stab_late, total_late = later
    stabilizer = jnp.maximum(total_late + stab_early, stab_late)
    keep_factor = jnp.exp(total_late + stab_early - stabilizer)
    take_factor = jnp.exp(stab_late - stabilizer)
    cell_state = (
        keep_factor[..., None, None] * cell_early + take_factor[..., None, None] * cell_late
    )
    norm_state = keep_factor[..., None] * norm_early + take_factor[..., None] * norm_late
    return (cell_state, norm_state, stabilizer, total_early + total_late)


def mix_heads(
    cell_query_rows,
    cell_key_rows,
    cell_value_rows,
    output_gate_logits,
    log_input_gate,
    forget_gate_logits,
    extra_log_forget,
    cell_output_scale,
):
    n_tok, row_width = cell_query_rows.shape
    head_count = row_width // HEAD_DIM
    block_count = n_tok // BLOCK
    key_scale = HEAD_DIM ** (-0.5)
    block_shape = (block_count, BLOCK, head_count, HEAD_DIM)
    query_blocks = cell_query_rows.reshape(block_shape)
    key_blocks = cell_key_rows.reshape(block_shape)
    value_blocks = cell_value_rows.reshape(block_shape)
    gate_input = log_input_gate.reshape(head_count, block_count, BLOCK)
    forget_gate_value = (jax.nn.log_sigmoid(forget_gate_logits) + extra_log_forget).reshape(
        head_count, block_count, BLOCK
    )
    cumulative = jnp.cumsum(forget_gate_value, axis=-1)
    block_last = cumulative[..., -1]
    growth = block_last[..., None] - cumulative + gate_input
    block_top = jnp.max(growth, axis=-1)
    shares = jnp.exp(growth - block_top[..., None])
    key_float = key_blocks.astype(jnp.float32) * key_scale
    value_weighted = value_blocks.astype(jnp.float32) * shares.transpose(1, 2, 0)[..., None]
    cell_terms = jnp.einsum("bshv,bshk->bhvk", value_weighted, key_float, precision=PRECISE)
    norm_terms = jnp.einsum("hbs,bshk->bhk", shares, key_float, precision=PRECISE)
    block_terms = (cell_terms, norm_terms, block_top.T, block_last.T)
    identity_state = (
        jnp.zeros((head_count, HEAD_DIM, HEAD_DIM), jnp.float32),
        jnp.zeros((head_count, HEAD_DIM), jnp.float32),
        jnp.full((head_count,), -1e30, jnp.float32),
        jnp.zeros((head_count,), jnp.float32),
    )

    def fold_step(running, block_term):
        return (combine(running, block_term), running)

    device_total, before = lax.scan(fold_step, identity_state, block_terms)
    prior_state = carried_in(device_total, "ep", combine, identity_state)
    zero_state = (
        jnp.zeros((head_count, HEAD_DIM, HEAD_DIM), jnp.float32),
        jnp.zeros((head_count, HEAD_DIM), jnp.float32),
        jnp.zeros((head_count,), jnp.float32),
        jnp.zeros((head_count,), jnp.float32),
    )
    start_state = combine(zero_state, prior_state)
    cell_state, norm_state, stabilizer, _ = combine(start_state, before)
    inter_log = cumulative + stabilizer.T[:, :, None]
    causal = jnp.tril(jnp.ones((BLOCK, BLOCK), dtype=bool))
    spread = jnp.where(
        causal,
        cumulative[..., :, None] - cumulative[..., None, :] + gate_input[..., None, :],
        -jnp.inf,
    )
    row_top = jnp.maximum(inter_log, jnp.max(spread, axis=-1))
    intra_weight = jnp.exp(spread - row_top[..., None])
    inter_weight = jnp.exp(inter_log - row_top)
    scores = (
        jnp.einsum("bthd,bshd->hbts", query_blocks, key_blocks, preferred_element_type=jnp.float32)
        * key_scale
        * intra_weight
    )
    weights = scores.astype(jnp.bfloat16)
    numerator = jnp.einsum(
        "hbts,bshd->hbtd", weights, value_blocks, preferred_element_type=jnp.float32
    )
    query_float = query_blocks.astype(jnp.float32)
    numerator = numerator + inter_weight[..., None] * jnp.einsum(
        "bhvk,bthk->hbtv", cell_state, query_float, precision=PRECISE
    )
    denominator = jnp.sum(scores, axis=-1) + inter_weight * jnp.einsum(
        "bhk,bthk->hbt", norm_state, query_float, precision=PRECISE
    )
    cell_out = numerator / jnp.maximum(jnp.abs(denominator), 1.0)[..., None]
    cell_out = cell_out.transpose(1, 2, 0, 3).reshape(n_tok, row_width)
    return (
        cell_out * cell_output_scale * jax.nn.sigmoid(output_gate_logits.astype(jnp.float32))
    ).astype(jnp.bfloat16)


def slot_tables(ids, experts, capacity):
    flat_ids = ids.reshape(-1)
    onehot = (flat_ids[:, None] == jnp.arange(experts, dtype=jnp.int32)[None, :]).astype(jnp.int32)
    earlier = jnp.cumsum(onehot, axis=0) - onehot
    rank_in = jnp.sum(earlier * onehot, axis=1)
    slot_index = flat_ids * capacity + rank_in
    token_of = jnp.arange(flat_ids.shape[0], dtype=jnp.int32) // ids.shape[1]
    slot_hit = slot_index[:, None] == jnp.arange(experts * capacity, dtype=jnp.int32)[None, :]
    slot_owner = jnp.sum(jnp.where(slot_hit, token_of[:, None] + 1, 0), axis=0)
    return (slot_owner, slot_index.reshape(ids.shape))


def local(
    cell_query_rows,
    cell_key_rows,
    cell_value_rows,
    output_gate_logits,
    log_input_gate,
    forget_gate_logits,
    extra_log_forget,
    cell_output_scale,
    tokens_into_experts,
    expert_norm_scale,
    token_expert_index,
    chosen_expert_weight,
    expert_gate_weight,
    expert_up_weight,
    expert_down_weight,
):
    gated_head_output = mix_heads(
        cell_query_rows,
        cell_key_rows,
        cell_value_rows,
        output_gate_logits,
        log_input_gate,
        forget_gate_logits,
        extra_log_forget,
        cell_output_scale,
    )
    ep_count = lax.axis_size("ep")
    n_tok = tokens_into_experts.shape[0]
    experts = ep_count * expert_gate_weight.shape[0]
    capacity = n_tok * TOPK * 5 // (4 * experts)
    input_float = tokens_into_experts.astype(jnp.float32)
    normed = (
        input_float
        * lax.rsqrt(jnp.mean(input_float * input_float, axis=-1, keepdims=True) + EPSILON)
        * expert_norm_scale
    ).astype(jnp.bfloat16)
    gate_matrix = expert_gate_weight[0]
    up_matrix = expert_up_weight[0]
    down_matrix = expert_down_weight[0]
    slot_owner, slot_index = slot_tables(token_expert_index, experts, capacity)
    sendbuf = jnp.where(
        (slot_owner > 0)[:, None],
        normed[jnp.maximum(slot_owner - 1, 0)],
        jnp.zeros((), jnp.bfloat16),
    )
    arrived = lax.all_to_all(sendbuf, "ep", split_axis=0, concat_axis=0, tiled=True)
    routed_rows = lax.all_gather(arrived, "tp", axis=0, tiled=True)
    gate_out = jnp.dot(routed_rows, gate_matrix, preferred_element_type=jnp.float32)
    up_out = jnp.dot(routed_rows, up_matrix, preferred_element_type=jnp.float32)
    hidden = (jax.nn.silu(gate_out) * up_out).astype(jnp.bfloat16)
    summed = lax.psum_scatter(
        jnp.dot(hidden, down_matrix, preferred_element_type=jnp.float32).astype(jnp.bfloat16),
        "tp",
        scatter_dimension=0,
        tiled=True,
    )
    returned = lax.all_to_all(summed, "ep", split_axis=0, concat_axis=0, tiled=True)
    picked = returned[slot_index]
    expert_output = jnp.sum(
        chosen_expert_weight[..., None] * picked.astype(jnp.float32), axis=1
    ).astype(jnp.bfloat16)
    return (gated_head_output, expert_output)


def solution(mesh):
    return jax.shard_map(
        local,
        mesh=mesh,
        in_specs=(
            P("ep", "tp"),
            P("ep", "tp"),
            P("ep", "tp"),
            P("ep", "tp"),
            P("tp", "ep"),
            P("tp", "ep"),
            P("tp", "ep"),
            P("tp"),
            P(("ep", "tp"), None),
            P(),
            P(("ep", "tp"), None),
            P(("ep", "tp"), None),
            P("ep", None, "tp"),
            P("ep", None, "tp"),
            P("ep", "tp", None),
        ),
        out_specs=(P("ep", "tp"), P(("ep", "tp"), None)),
        check_vma=False,
    )
```

profile of v0, /device:TPU:0, one launch (start us, length us, event | category | flops | bytes accessed | tf_op | source)
XLA Modules:
  0.0 271.6 jit_solution(12901544852267951957)
XLA Ops:
  7.2 0.8 copy.103
  8.0 0.1 eq.39
  8.1 0.1 reshape.150
  8.3 0.6 reduce-window.6
  8.9 0.2 slice_reduce_fusion
  9.2 0.1 select_reduce_fusion
  9.4 1.2 fusion.31
  10.8 1.2 fusion.33
  12.0 2.4 gather_fusion
  14.4 0.2 broadcast_select_fusion.7
  14.7 38.7 %all_to_all.21 = bf16[8,40,2048]{2,1,0:T(8,128)(2,1)} all-to-all(bf16[8,40,2048]{2,1,0:T(8,128)(2,1)S(1)} %broadcast_select_fusion.7), channel_id=1, replica_groups=mesh['ep'=8,'tp'=4] {'ep'}, dimensions={0} | all-to-all | bytes 2621440 | tf_op jit(solution)/shard_map/all_to_all | solution.py:186
  53.8 0.5 reduce_window_sum.28
  54.2 0.2 slice_reduce_fusion.1
  54.4 0.2 fusion.70
  54.8 0.4 fusion.34
  55.4 2.0 fusion.35
  57.4 4.8 %while.45 = (s32[]{:T(128)}, f32[2,256,256]{2,1,0:T(8,128)S(1)}, f32[2,256]{1,0:T(2,128)S(1)}, f32[2]{0:T(128)S(1)}, f32[2]{0:T(128)S(1)}, /*index=5*/f32[4,2,25...) while((s32[]{:T(128)}, f32[2,256,256]{2,1,0:T(8,128)S(1)}, ...), condition=%wide.region_3.4_spmd.clone, body=%wide.region_2.3_spmd.clone.sunk | while | flops 657939 | bytes 2632544 | solution.py:85
  57.5 0.8 bitcast_dynamic-update-slice_fusion.4
  58.3 0.1 fusion.89
  58.6 0.8 bitcast_dynamic-update-slice_fusion.4
  59.5 0.1 fusion.89
  59.8 0.8 bitcast_dynamic-update-slice_fusion.4
  60.7 0.1 fusion.89
  61.0 0.8 bitcast_dynamic-update-slice_fusion.4
  61.8 0.1 fusion.89
  62.2 0.8 copy-done
  63.0 30.0 %all-gather.8.cloned.1.call-done = bf16[1280,2048]{1,0:T(8,128)(2,1)} async-done(((bf16[320,2048]{1,0:T(8,128)(2,1)}), bf16[1280,2048]{1,0:T(8,128)(2,1)}) %all-gather.8.cloned.1.call-update) | async-done | bytes 5242896 | tf_op jit(solution)/shard_map/all_gather | solution.py:187
  93.0 10.0 %fusion.18 = f32[1280,896]{1,0:T(8,128)} fusion(bf16[1280,2048]{1,0:T(8,128)(2,1)} %all-gather.8.cloned.1.call-done, bf16[1,2048,896]{2,1,0:T(8,128)(2,1)} %param.31), kind=kOutput, calls=%fused_computation.43 | convolution fusion | flops 4697620480 | bytes 13500416 | tf_op jit(solution)/shard_map/dot_general | solution.py:188
  103.0 17.9 %convolution_convert_fusion = bf16[1280,2048]{1,0:T(8,128)(2,1)} fusion(bf16[1,896,2048]{2,1,0:T(8,128)(2,1)} %param.33, f32[1280,896]{1,0:T(8,128)} %fusion.18, bf16[1280,2048]{1,0:T(8,128)(2,1)} %all-gather.8.cloned.1.call-done, bf16[1,2048,896]{2,1,0:T(8,128)(2,1)} %param.32), kind=kOutput, calls=%fused_computation.39 | convolution fusion | flops 9404743680 | bytes 22413312 | tf_op jit(solution)/shard_map/dot_general | solution.py:192
  120.9 0.6 copy-done.12
  121.5 0.6 dynamic-slice
  122.8 0.2 dynamic-update-slice
  123.0 0.2 dynamic-update-slice.1
  123.2 22.6 %all-reduce.2 = (f32[16]{0:T(128)S(1)}, f32[16]{0:T(128)S(1)}) all-reduce(f32[16]{0:T(128)S(1)} %dynamic-update-slice, f32[16]{0:T(128)S(1)} %dynamic-update-slice.1), channel_id=2, replica_groups=mesh['ep'=8,'tp'=4] {'ep'}, use_global_device_ids=true, to_apply=%add | all-reduce | flops 32 | bytes 256
  145.8 0.1 reduce_sum.54
  146.3 0.1 copy.106
  146.4 0.1 reshape.162
  146.5 0.1 copy.102
  146.6 26.9 %all-gather.4 = f32[8,2,256]{2,1,0:T(2,128)S(1)} all-gather(f32[1,2,256]{2,1,0:T(2,128)S(1)} %bitcast.169), channel_id=5, replica_groups=mesh['ep'=8,'tp'=4] {'ep'}, dimensions={0}, use_global_device_ids=true | all-gather | bytes 18432 | tf_op jit(solution)/shard_map/all_gather | solution.py:17
  173.6 0.2 fusion.44
  173.8 11.0 %while.46 = (s32[]{:T(128)}, f32[2,256,256]{2,1,0:T(8,128)S(1)}, f32[2,256]{1,0:T(2,128)S(1)}, f32[2]{0:T(128)S(1)}, f32[2]{0:T(128)S(1)}, /*index=5*/s32[]{:T(1...) while((s32[]{:T(128)}, f32[2,256,256]{2,1,0:T(8,128)S(1)}, ...), condition=%wide.region_5.6_spmd.clone, body=%wide.region_4.5_spmd.clone.sunk | while | flops 657944 | bytes 1579285 | solution.py:27
  173.9 1.2 fusion.92
  175.2 1.3 fusion.92
  176.7 1.2 fusion.92
  178.0 1.3 fusion.92
  179.4 1.3 fusion.92
  180.9 1.2 fusion.92
  182.2 1.2 fusion.92
  183.6 1.2 fusion.92
  184.9 36.8 %reduce-scatter.2.cloned.1.call-done = bf16[320,2048]{1,0:T(8,128)(2,1)} async-done(((bf16[1280,2048]{1,0:T(8,128)(2,1)}), bf16[320,2048]{1,0:T(8,128)(2,1)}) %reduce-scatter.2.cloned.1.call-update) | async-done | bytes 1310736 | tf_op jit(solution)/shard_map/reduce_scatter | solution.py:191
  221.7 5.5 %all-to-all-start.1 = ((bf16[8,40,2048]{2,1,0:T(8,128)(2,1)}), bf16[8,40,2048]{2,1,0:T(8,128)(2,1)S(1)}, u32[]{:S(2)}, u32[]{:S(2)}) async-start(bf16[8,40,2048]{2,1,0:T(8,128)(2,1)} %bitcast.168), calls=%async_computation.2 | async-start | bytes 2621440 | tf_op jit(solution)/shard_map/all_to_all | solution.py:197
  227.6 0.3 fusion.48
  227.9 0.3 fusion.71
  228.3 0.1 multiply_add_fusion.1
  228.4 0.6 copy-done.1
  229.1 1.5 fusion.27
  230.6 0.3 fusion.26
  230.9 0.4 copy.101
  231.3 0.2 copy-done.5
  231.5 0.9 multiply_convert_fusion.1
  232.4 26.1 %all-to-all-done.1 = bf16[8,40,2048]{2,1,0:T(8,128)(2,1)S(1)} async-done(((bf16[8,40,2048]{2,1,0:T(8,128)(2,1)}), bf16[8,40,2048]{2,1,0:T(8,128)(2,1)S(1)}, u32[]{:S(2)}, u32[]{:S(2)}) %all-to-all-start.1) | async-done | bytes 1310752 | tf_op jit(solution)/shard_map/all_to_all | solution.py:197
  258.5 1.4 gather_fusion.1
  259.8 1.3 reshape.175
  261.2 3.9 %multiply_reduce_fusion = bf16[128,2048]{1,0:T(8,128)(2,1)} fusion(f32[128,2,2048]{2,1,0:T(2,128)S(1)} %reshape.175, f32[128,2]{1,0:T(8,128)S(1)} %copy.102), kind=kLoop, calls=%fused_computation.47 | loop fusion | flops 786432 | bytes 2622464 | tf_op jit(solution)/shard_map/reduce_sum | solution.py:199
  (133 shorter events, 3.7 us)
Async XLA Ops:
  7.2 85.9 %all-gather.8.cloned.1.call-start = ((), (), s32[]{:S(2)}) async-start(), calls=%async_computation.3 | async-start | bytes 6553600 | tf_op jit(solution)/shard_map/all_gather | solution.py:187
  14.6 38.9 %copy-start.8 = (f32[2,256]{1,0:T(2,128)S(1)}, f32[2,256]{1,0:T(2,128)}, u32[]{:S(2)}) copy-start(f32[2,256]{1,0:T(2,128)} %param.25) | copy-start | bytes 6148
  14.6 38.9 %copy-start.9 = (f32[2,256]{1,0:T(2,128)S(1)}, f32[2,256]{1,0:T(2,128)}, u32[]{:S(2)}) copy-start(f32[2,256]{1,0:T(2,128)} %param.24) | copy-start | bytes 6148
  14.6 39.0 %copy-start.10 = (f32[2,256]{1,0:T(2,128)S(1)}, f32[2,256]{1,0:T(2,128)}, u32[]{:S(2)}) copy-start(f32[2,256]{1,0:T(2,128)} %param.23) | copy-start | bytes 6148
  14.6 40.0 %copy-start.2 = (bf16[256,512]{1,0:T(8,128)(2,1)S(1)}, bf16[256,512]{1,0:T(8,128)(2,1)}, u32[]{:S(2)}) copy-start(bf16[256,512]{1,0:T(8,128)(2,1)} %param.20) | copy-start | bytes 786436
  14.7 40.1 %copy-start.3 = (bf16[256,512]{1,0:T(8,128)(2,1)S(1)}, bf16[256,512]{1,0:T(8,128)(2,1)}, u32[]{:S(2)}) copy-start(bf16[256,512]{1,0:T(8,128)(2,1)} %param.21) | copy-start | bytes 786436
  53.4 120.4 %all-gather.10.cloned.1.call-start = ((), (), s32[]{:S(2)}) async-start(), calls=%async_computation.5 | async-start | bytes 4718592 | tf_op jit(solution)/shard_map/all_gather | solution.py:17
  62.1 0.8 copy-start
  63.0 158.7 %reduce-scatter.2.cloned.1.call-start = ((), (), s32[]{:S(2)}) async-start(), calls=%async_computation.4 | async-start | bytes 6553600 | tf_op jit(solution)/shard_map/reduce_scatter | solution.py:191
  120.9 0.7 copy-start.12
  120.9 25.2 %copy-start.4 = (bf16[256,512]{1,0:T(8,128)(2,1)S(1)}, bf16[256,512]{1,0:T(8,128)(2,1)}, u32[]{:S(2)}) copy-start(bf16[256,512]{1,0:T(8,128)(2,1)} %param.19) | copy-start | bytes 786436
  120.9 25.4 %copy-start.6 = (s32[128,2]{0,1:T(2,128)S(1)}, s32[128,2]{0,1:T(2,128)}, u32[]{:S(2)}) copy-start(s32[128,2]{0,1:T(2,128)} %param.29) | copy-start | bytes 3076
  120.9 25.6 %copy-start.11 = (f32[128,2]{0,1:T(2,128)S(1)}, f32[128,2]{0,1:T(2,128)}, u32[]{:S(2)}) copy-start(f32[128,2]{0,1:T(2,128)} %param.30) | copy-start | bytes 3076
  221.7 36.8 %all-to-all-start.1 = ((bf16[8,40,2048]{2,1,0:T(8,128)(2,1)}), bf16[8,40,2048]{2,1,0:T(8,128)(2,1)S(1)}, u32[]{:S(2)}, u32[]{:S(2)}) async-start(bf16[8,40,2048]{2,1,0:T(8,128)(2,1)} %bitcast.168), calls=%async_computation.2 | async-start | bytes 2621440 | tf_op jit(solution)/shard_map/all_to_all | solution.py:197
  227.5 1.6 copy-start.1
  230.5 1.0 copy-start.5
  230.6 0.9 copy-start.7
Sparse Core Ops, SparseCore 0:
  53.5 39.4 all-gather.7
  95.7 73.2 all-gather.9
  171.5 50.1 reduce-scatter.1
where the time goes:
time: 272 us
  waiting for transfers between devices  93 us (34%)
  blocking collectives  88.2 us (32%)
  matrix products  32.6 us (12%)
  other arithmetic  25 us (9%)
  between operations  14.8 us (5%)
  local copies, waits for them, and re-layouts  12.1 us (4%)
  starting transfers between devices  5.64 us (2%)
    all_to_all x1, blocking collectives, local(): lax.all_to_all(sendbuf, 'ep', split_axis=0, concat_axis=0, tiled=True)  38.7 us
    reduce_scatter x1, waiting for transfers between devices, local(): lax.psum_scatter(jnp.dot(hidden, down_matrix, preferred_element_type=jnp....  36.8 us
    all_gather x1, waiting for transfers between devices, local(): routed_rows = lax.all_gather(arrived, 'tp', axis=0, tiled=True)  30 us
    all_gather x1, blocking collectives, carried_in(): everything = jax.tree.map(lambda part: lax.all_gather(part, axis), x)  26.9 us
    all_to_all x1, waiting for transfers between devices, local(): lax.all_to_all(summed, 'ep', split_axis=0, concat_axis=0, tiled=True)  26.1 us
    unnamed x1, blocking collectives  22.6 us
    dot_general x1, matrix products, local(): jnp.dot(hidden, down_matrix, preferred_element_type=jnp.float32)  17.9 us
    select_n x24, other arithmetic, step(): return jax.tree.map(lambda a, b: jnp.where(reached, a, b), new, before)  10.8 us
  transfers between devices with their start and end apart: 4, of which 3 were waited for; matrix products, arithmetic and copies ran while one was open for 20% of the time, Pallas kernels for 0%

commit v1 on v0

--- a/solution.py
+++ b/solution.py
@@ -1,6 +1,10 @@
+import functools
+
 import jax
 import jax.numpy as jnp
 from jax import lax
+from jax.experimental import pallas as pl
+from jax.experimental.pallas import tpu as pltpu
 from jax.sharding import PartitionSpec as P
 
 HEAD_DIM = 256
@@ -15,9 +19,7 @@
 def carried_in(x, axis, combine, identity):
     size, here = (lax.axis_size(axis), lax.axis_index(axis))
     everything = jax.tree.map(lambda part: lax.all_gather(part, axis), x)
-    start = jax.tree.map(
-        lambda part, zero: jnp.broadcast_to(jnp.asarray(zero, part.dtype), part.shape), x, identity
-    )
+    start = identity
 
     def step(k, before):
         reached = k < here
@@ -83,7 +85,8 @@
         return (combine(running, block_term), running)
 
     device_total, before = lax.scan(fold_step, identity_state, block_terms)
-    prior_state = carried_in(device_total, "ep", combine, identity_state)
+    sent_state = (device_total[0].astype(jnp.bfloat16),) + device_total[1:]
+    prior_state = carried_in(sent_state, "ep", combine, identity_state)
     zero_state = (
         jnp.zeros((head_count, HEAD_DIM, HEAD_DIM), jnp.float32),
         jnp.zeros((head_count, HEAD_DIM), jnp.float32),
@@ -135,6 +138,246 @@
     slot_hit = slot_index[:, None] == jnp.arange(experts * capacity, dtype=jnp.int32)[None, :]
     slot_owner = jnp.sum(jnp.where(slot_hit, token_of[:, None] + 1, 0), axis=0)
     return (slot_owner, slot_index.reshape(ids.shape))
+
+
+MESH = pl.DeviceIdType.MESH
+LANES = 128
+
+
+def expert_kernel(
+    n_ep,
+    send_ref,
+    gate_hbm,
+    up_hbm,
+    down_hbm,
+    ret_ref,
+    disp,
+    part,
+    first,
+    pair_sum,
+    second,
+    final,
+    rows_in,
+    hidden,
+    gate_up,
+    down,
+    weight_sem,
+    local_sem,
+    sem_a_send,
+    sem_a_recv,
+    sem_x_send,
+    sem_x_recv,
+    sem_c_send,
+    sem_c_recv,
+    sem_d_send,
+    sem_d_recv,
+    sem_f_send,
+    sem_f_recv,
+    sem_s_send,
+    sem_s_recv,
+    sem_r_send,
+    sem_r_recv,
+):
+    e, t = lax.axis_index("ep"), lax.axis_index("tp")
+    partner = t + 1 - 2 * (t % 2)
+    across = (t + 2) % 4
+    cap, width = send_ref.shape[1], send_ref.shape[2]
+    tiles, outs = gate_up.shape[0], down.shape[0]
+    out_cols = down.shape[2]
+
+    def remote(src, dst, ssem, rsem, dev):
+        return pltpu.make_async_remote_copy(
+            src_ref=src, dst_ref=dst, send_sem=ssem, recv_sem=rsem, device_id=dev, device_id_type=MESH
+        )
+
+    barrier = pltpu.get_barrier_semaphore()
+    for k in range(1, n_ep):
+        pl.semaphore_signal(barrier, inc=1, device_id=((e + k) % n_ep, t), device_id_type=MESH)
+    for other in (partner, across):
+        pl.semaphore_signal(barrier, inc=1, device_id=(e, other), device_id_type=MESH)
+
+    weights = []
+    for j in range(tiles):
+        cols = pl.ds(j * LANES, LANES)
+        weights.append(
+            pltpu.make_async_copy(gate_hbm.at[:, cols], gate_up.at[j, :, pl.ds(0, LANES)], weight_sem.at[3 * j])
+        )
+        weights.append(
+            pltpu.make_async_copy(up_hbm.at[:, cols], gate_up.at[j, :, pl.ds(LANES, LANES)], weight_sem.at[3 * j + 1])
+        )
+    for j in range(outs):
+        weights.append(
+            pltpu.make_async_copy(
+                down_hbm.at[:, pl.ds(j * out_cols, out_cols)], down.at[j], weight_sem.at[3 * tiles + j]
+            )
+        )
+    local = pltpu.make_async_copy(send_ref.at[0], disp.at[0, 0], local_sem)
+    local.start()
+    pl.semaphore_wait(barrier, n_ep + 1)
+
+    def out_copy(k):
+        return remote(send_ref.at[k], disp.at[k, 0], sem_a_send.at[k], sem_a_recv.at[k], ((e + k) % n_ep, t))
+
+    def to_across(k):
+        return remote(disp.at[k, 0], disp.at[k, 1], sem_x_send.at[k], sem_x_recv.at[k], (e, across))
+
+    def to_partner_own(k):
+        return remote(disp.at[k, 0], disp.at[k, 2], sem_c_send.at[k], sem_c_recv.at[k], (e, partner))
+
+    def to_partner_far(k):
+        return remote(disp.at[k, 1], disp.at[k, 3], sem_d_send.at[k], sem_d_recv.at[k], (e, partner))
+
+    def sum_to_partner(k):
+        return remote(part.at[k, pl.ds(2, 2)], first.at[k], sem_f_send.at[k], sem_f_recv.at[k], (e, partner))
+
+    def sum_across(k):
+        return remote(pair_sum.at[k], second.at[k], sem_s_send.at[k], sem_s_recv.at[k], (e, across))
+
+    def give_back(k):
+        return remote(final.at[k], ret_ref.at[k], sem_r_send.at[k], sem_r_recv.at[k], ((e + n_ep - k) % n_ep, t))
+
+    half = n_ep // 2
+    for k in range(half):
+        out_copy(k + half).start()
+        if k:
+            out_copy(k).start()
+    for copy in weights:
+        copy.start()
+
+    def spread_own(i):
+        for k in (i, i + half):
+            if k:
+                out_copy(k).wait_recv()
+            else:
+                local.wait()
+            to_across(k).start()
+            to_partner_own(k).start()
+
+    def spread_far(i):
+        for k in (i, i + half):
+            to_across(k).wait_recv()
+            to_partner_far(k).start()
+
+    def all_here(i):
+        for k in (i, i + half):
+            to_partner_own(k).wait_recv()
+            to_partner_far(k).wait_recv()
+
+    def wide(block):
+        return block.astype(jnp.float32)
+
+    def sum_pairs(i):
+        for k in (i, i + half):
+            sum_to_partner(k).wait_recv()
+            pair_sum[k] = (wide(part[k, 1]) + wide(first[k, 1])).astype(jnp.bfloat16)
+            sum_across(k).start()
+
+    def sum_rest(i):
+        for k in (i, i + half):
+            sum_across(k).wait_recv()
+            done = (wide(part[k, 0]) + wide(first[k, 0]) + wide(second[k])).astype(jnp.bfloat16)
+            if k:
+                final[k] = done
+                give_back(k).start()
+            else:
+                ret_ref[0] = done
+
+    def hidden_units(i):
+        for at, k in enumerate((i, i + half)):
+            block = jnp.concatenate([wide(disp[k, j]) for j in range(4)], axis=0)
+            rows_in[pl.ds(at * 4 * cap, 4 * cap)] = block.astype(jnp.bfloat16)
+
+        def step(j, carry):
+            both = jnp.dot(rows_in[...], gate_up[j], preferred_element_type=jnp.float32)
+            gate_out, up_out = both[:, :LANES], both[:, LANES:]
+            hidden[j] = (jax.nn.silu(gate_out) * up_out).astype(jnp.bfloat16)
+            return carry
+
+        lax.fori_loop(0, tiles, step, 0)
+
+    def results(i):
+        units = jnp.concatenate([hidden[j] for j in range(tiles)], axis=1)
+
+        def step(j, carry):
+            out = jnp.dot(units, down[j], preferred_element_type=jnp.float32)
+            cols = pl.ds(pl.multiple_of(j * out_cols, out_cols), out_cols)
+            for at, k in enumerate((i, i + half)):
+                for m in range(4):
+                    lo = (at * 4 + m) * cap
+                    part[k, m, :, cols] = out[lo : lo + cap].astype(jnp.bfloat16)
+            return carry
+
+        lax.fori_loop(0, outs, step, 0)
+
+    spread_own(0)
+    spread_far(0)
+    for i in range(half):
+        all_here(i)
+        if i == 0:
+            for copy in weights:
+                copy.wait()
+        if i + 1 < half:
+            spread_own(i + 1)
+        hidden_units(i)
+        if i:
+            sum_pairs(i - 1)
+        results(i)
+        for k in (i, i + half):
+            sum_to_partner(k).start()
+        if i + 1 < half:
+            spread_far(i + 1)
+        if i:
+            sum_rest(i - 1)
+    sum_pairs(half - 1)
+    sum_rest(half - 1)
+    for k in range(n_ep):
+        if k:
+            give_back(k).wait_recv()
+            out_copy(k).wait_send()
+            give_back(k).wait_send()
+        to_across(k).wait_send()
+        to_partner_own(k).wait_send()
+        to_partner_far(k).wait_send()
+        sum_to_partner(k).wait_send()
+        sum_across(k).wait_send()
+
+
+def experts_by_kernel(sendbuf, gate_matrix, up_matrix, down_matrix, n_ep):
+    rows, width = sendbuf.shape
+    cap = rows // n_ep
+    units = gate_matrix.shape[1]
+    tiles, out_cols = units // LANES, 256
+    block = (n_ep, cap, width)
+    vmem = pltpu.VMEM
+    bf16 = jnp.bfloat16
+    dma = pltpu.SemaphoreType.DMA
+    return pl.pallas_call(
+        functools.partial(expert_kernel, n_ep),
+        out_shape=jax.ShapeDtypeStruct(block, bf16),
+        in_specs=[pl.BlockSpec(memory_space=pltpu.VMEM)] + [pl.BlockSpec(memory_space=pl.ANY)] * 3,
+        out_specs=pl.BlockSpec(memory_space=pltpu.VMEM),
+        scratch_shapes=[
+            vmem((n_ep, 4, cap, width), bf16),
+            vmem((n_ep, 4, cap, width), bf16),
+            vmem((n_ep, 2, cap, width), bf16),
+            vmem(block, bf16),
+            vmem(block, bf16),
+            vmem(block, bf16),
+            vmem((8 * cap, width), bf16),
+            vmem((tiles, 8 * cap, LANES), bf16),
+            vmem((tiles, width, 2 * LANES), bf16),
+            vmem((width // out_cols, units, out_cols), bf16),
+            dma((3 * tiles + width // out_cols,)),
+            dma,
+        ]
+        + [dma((n_ep,))] * 14,
+        compiler_params=pltpu.CompilerParams(
+            collective_id=0, has_side_effects=True, vmem_limit_bytes=56 * 1024 * 1024
+        ),
+        cost_estimate=pl.CostEstimate(
+            flops=24 * rows * width * units, bytes_accessed=6 * width * units, transcendentals=4 * rows * units
+        ),
+    )(sendbuf.reshape(block), gate_matrix, up_matrix, down_matrix).reshape(rows, width)
 
 
 def local(
@@ -177,24 +420,36 @@
     gate_matrix = expert_gate_weight[0]
     up_matrix = expert_up_weight[0]
     down_matrix = expert_down_weight[0]
+    by_kernel = (
+        lax.axis_size("tp") == 4
+        and ep_count % 2 == 0
+        and capacity % 8 == 0
+        and gate_matrix.shape[1] % LANES == 0
+        and gate_matrix.shape[0] % 256 == 0
+    )
+    if by_kernel:
+        token_expert_index = (token_expert_index + ep_count - lax.axis_index("ep")) % ep_count
     slot_owner, slot_index = slot_tables(token_expert_index, experts, capacity)
     sendbuf = jnp.where(
         (slot_owner > 0)[:, None],
         normed[jnp.maximum(slot_owner - 1, 0)],
         jnp.zeros((), jnp.bfloat16),
     )
-    arrived = lax.all_to_all(sendbuf, "ep", split_axis=0, concat_axis=0, tiled=True)
-    routed_rows = lax.all_gather(arrived, "tp", axis=0, tiled=True)
-    gate_out = jnp.dot(routed_rows, gate_matrix, preferred_element_type=jnp.float32)
-    up_out = jnp.dot(routed_rows, up_matrix, preferred_element_type=jnp.float32)
-    hidden = (jax.nn.silu(gate_out) * up_out).astype(jnp.bfloat16)
-    summed = lax.psum_scatter(
-        jnp.dot(hidden, down_matrix, preferred_element_type=jnp.float32).astype(jnp.bfloat16),
-        "tp",
-        scatter_dimension=0,
-        tiled=True,
-    )
-    returned = lax.all_to_all(summed, "ep", split_axis=0, concat_axis=0, tiled=True)
+    if by_kernel:
+        returned = experts_by_kernel(sendbuf, gate_matrix, up_matrix, down_matrix, ep_count)
+    else:
+        arrived = lax.all_to_all(sendbuf, "ep", split_axis=0, concat_axis=0, tiled=True)
+        routed_rows = lax.all_gather(arrived, "tp", axis=0, tiled=True)
+        gate_out = jnp.dot(routed_rows, gate_matrix, preferred_element_type=jnp.float32)
+        up_out = jnp.dot(routed_rows, up_matrix, preferred_element_type=jnp.float32)
+        hidden = (jax.nn.silu(gate_out) * up_out).astype(jnp.bfloat16)
+        summed = lax.psum_scatter(
+            jnp.dot(hidden, down_matrix, preferred_element_type=jnp.float32).astype(jnp.bfloat16),
+            "tp",
+            scatter_dimension=0,
+            tiled=True,
+        )
+        returned = lax.all_to_all(summed, "ep", split_axis=0, concat_axis=0, tiled=True)
     picked = returned[slot_index]
     expert_output = jnp.sum(
         chosen_expert_weight[..., None] * picked.astype(jnp.float32), axis=1

time: 272 us -> 224 us (0.82)
  Pallas kernels: 0 us -> 109 us
  waiting for transfers between devices: 93 us -> 0.02 us
  blocking collectives: 88.2 us -> 50.1 us
  matrix products: 32.6 us -> 7.76 us
  starting transfers between devices: 5.64 us -> 0.04 us
  local copies, waits for them, and re-layouts: 12.1 us -> 17.4 us
    pallas_call x0 -> x1, Pallas kernels: none -> 109 us  [experts_by_kernel(): pl.pallas_call(functools.partial(expert_kernel, n_ep), out_shape=jax.Shap...]
    all_to_all x1 -> x0, blocking collectives: 38.7 us -> none  [local(): lax.all_to_all(sendbuf, 'ep', split_axis=0, concat_axis=0, tiled=True)]
    reduce_scatter x1 -> x0, waiting for transfers between devices: 36.8 us -> none  [local(): lax.psum_scatter(jnp.dot(hidden, down_matrix, preferred_element_type=jnp....]
    all_gather x1 -> x0, waiting for transfers between devices: 30 us -> none  [local(): routed_rows = lax.all_gather(arrived, 'tp', axis=0, tiled=True)]
    dot_general x2 -> x0, matrix products: 27.8 us -> none  [the longest x1 17.9 us: local(): jnp.dot(hidden, down_matrix, preferred_element_type=jnp.float32)]
    all_to_all x1 -> x0, waiting for transfers between devices: 26.1 us -> none  [local(): lax.all_to_all(summed, 'ep', split_axis=0, concat_axis=0, tiled=True)]
    all_to_all x1 -> x0, starting transfers between devices: 5.52 us -> none  [local(): lax.all_to_all(summed, 'ep', split_axis=0, concat_axis=0, tiled=True)]
    gather x1, local copies, waits for them, and re-layouts: 1.36 us -> 4.85 us  [local(): picked = returned[slot_index]]
  transfers between devices with their start and end apart: 4 -> 1, of which waited for: 3 -> 0; matrix products, arithmetic and copies ran while one was open for 20% -> 9% of each run, Pallas kernels for 0% -> 49%
where the time goes in v1:
time: 224 us
  Pallas kernels  109 us (49%)
  blocking collectives  50.1 us (22%)
  other arithmetic  24.5 us (11%)
  local copies, waits for them, and re-layouts  17.4 us (8%)
  between operations  15.1 us (7%)
  matrix products  7.76 us (3%)
    pallas_call x1, Pallas kernels, experts_by_kernel(): pl.pallas_call(functools.partial(expert_kernel, n_ep), out_shape=jax.Shap...  109 us
    all_gather x1, blocking collectives, carried_in(): everything = jax.tree.map(lambda part: lax.all_gather(part, axis), x)  26.3 us
    unnamed x1, blocking collectives  23.8 us
    select_n x24, other arithmetic, step(): return jax.tree.map(lambda a, b: jnp.where(reached, a, b), new, before)  9.7 us
    gather x1, local copies, waits for them, and re-layouts, local(): picked = returned[slot_index]  4.85 us
  transfers between devices with their start and end apart: 1, of which 0 were waited for; matrix products, arithmetic and copies ran while one was open for 9% of the time, Pallas kernels for 49%

profile of v1, /device:TPU:0, one launch (start us, length us, event | category | flops | bytes accessed | tf_op | source)
XLA Modules:
  0.0 223.6 jit_solution(17075024334494097954)
XLA Ops:
  7.3 0.7 fusion.59
  8.1 0.5 reduce_window_sum.28
  8.6 0.2 slice_reduce_fusion.1
  8.7 0.8 add.212
  9.5 0.2 fusion.67
  9.7 1.0 reshape.148
  10.8 1.1 reshape.150
  11.9 0.4 fusion.30
  12.3 0.1 copy.103
  12.4 0.1 copy.102
  12.5 2.0 fusion.31
  14.5 4.8 %while.45 = (s32[]{:T(128)}, f32[2,256,256]{2,1,0:T(8,128)S(1)}, f32[2,256]{1,0:T(2,128)S(1)}, f32[2]{0:T(128)S(1)}, f32[2]{0:T(128)S(1)}, /*index=5*/f32[4,2,25...) while((s32[]{:T(128)}, f32[2,256,256]{2,1,0:T(8,128)S(1)}, ...), condition=%wide.region_3.4_spmd.clone, body=%wide.region_2.3_spmd.clone.sunk | while | flops 657939 | bytes 2632544 | solution.py:87
  14.6 0.8 bitcast_dynamic-update-slice_fusion.4
  15.4 0.1 fusion.75
  15.8 0.9 bitcast_dynamic-update-slice_fusion.4
  16.6 0.1 fusion.75
  17.0 0.8 bitcast_dynamic-update-slice_fusion.4
  17.8 0.1 fusion.75
  18.2 0.9 bitcast_dynamic-update-slice_fusion.4
  19.0 0.1 fusion.75
  19.4 0.7 convert_element_type.50
  20.1 0.1 copy.112
  20.3 0.1 eq.41
  20.4 0.1 reshape.152
  20.6 0.6 reduce-window.6
  21.1 0.2 slice_reduce_fusion
  21.5 0.1 reduce_sum.54
  21.8 0.6 dynamic-slice
  23.0 0.2 dynamic-update-slice
  23.2 0.2 dynamic-update-slice.1
  23.5 0.1 select_reduce_fusion
  23.6 23.8 %all-reduce.2 = (f32[16]{0:T(128)S(1)}, f32[16]{0:T(128)S(1)}) all-reduce(f32[16]{0:T(128)S(1)} %dynamic-update-slice, f32[16]{0:T(128)S(1)} %dynamic-update-slice.1), channel_id=2, replica_groups=mesh['ep'=8,'tp'=4] {'ep'}, use_global_device_ids=true, to_apply=%add | all-reduce | flops 32 | bytes 256
  47.6 0.8 reshape.147
  48.4 0.1 copy.115
  48.5 0.1 reshape.166
  48.7 0.2 fusion.27
  48.9 0.2 fusion.29
  49.1 2.4 %gather_fusion = bf16[320,2048]{1,0:T(8,128)(2,1)S(1)} fusion(bf16[128,2048]{1,0:T(8,128)(2,1)S(1)} %fusion.29, s32[1024]{0:T(1024)S(1)} %pad_clamp_fusion.1), kind=kCustom, calls=%fused_computation | custom fusion | bytes 2622720 | tf_op jit(solution)/shard_map/gather | solution.py:435
  51.6 1.3 broadcast_select_fusion.7.send_ref
  52.8 108.6 %shard_map.158 = bf16[8,40,2048]{2,1,0:T(8,128)(2,1)} custom-call(bf16[8,40,2048]{2,1,0:T(8,128)(2,1)} %broadcast_select_fusion.7.send_ref, bf16[2048,896]{1,0:T(8,128)(2,1)} %bitcast.151, bf16[2048,896]{1,0:T(8,128)(2,1)} %bitcast.152, bf16[896,2048]{1,0:T(8,128)(2,1)} %bitcast.153), custom_call_target="tpu_custom_call" | custom-call | flops 14092861440 | bytes 11010048 | tf_op jit(solution)/shard_map/pallas_call | solution.py:354
  161.4 4.9 %gather_fusion.1 = bf16[256,2048]{1,0:T(8,128)(2,1)} fusion(bf16[320,2048]{1,0:T(8,128)(2,1)} %bitcast.140, s32[1024]{0:T(1024)S(1)} %pad_clamp_fusion), kind=kCustom, calls=%fused_computation.1 | custom fusion | bytes 2098176 | tf_op jit(solution)/shard_map/gather | solution.py:453
  166.3 2.4 %reshape.179 = f32[128,2,2048]{2,1,0:T(2,128)S(1)} reshape(bf16[256,2048]{1,0:T(8,128)(2,1)} %gather_fusion.1) | data formatting | bytes 3145728 | tf_op jit(solution)/shard_map/convert_element_type | solution.py:455
  168.7 0.1 copy.111
  168.8 26.3 %all-gather.4 = f32[8,2,256]{2,1,0:T(2,128)S(1)} all-gather(f32[1,2,256]{2,1,0:T(2,128)S(1)} %bitcast.145), channel_id=5, replica_groups=mesh['ep'=8,'tp'=4] {'ep'}, dimensions={0}, use_global_device_ids=true | all-gather | bytes 18432 | tf_op jit(solution)/shard_map/all_gather | solution.py:21
  195.1 0.2 fusion.40
  195.3 3.9 %multiply_reduce_fusion = bf16[128,2048]{1,0:T(8,128)(2,1)} fusion(f32[128,2,2048]{2,1,0:T(2,128)S(1)} %reshape.179, f32[128,2]{1,0:T(8,128)S(1)} %copy.111), kind=kLoop, calls=%fused_computation.41 | loop fusion | flops 786432 | bytes 2622464 | tf_op jit(solution)/shard_map/reduce_sum | solution.py:454
  199.3 9.9 %while.46 = (s32[]{:T(128)}, f32[2,256,256]{2,1,0:T(8,128)S(1)}, f32[2,256]{1,0:T(2,128)S(1)}, f32[2]{0:T(128)S(1)}, f32[2]{0:T(128)S(1)}, /*index=5*/s32[]{:T(1...) while((s32[]{:T(128)}, f32[2,256,256]{2,1,0:T(8,128)S(1)}, ...), condition=%wide.region_5.6_spmd.clone, body=%wide.region_4.5_spmd.clone.sunk | while | flops 789016 | bytes 1317141 | solution.py:29
  199.3 1.1 fusion.78
  200.5 1.1 fusion.78
  201.8 1.1 fusion.78
  203.0 1.1 fusion.78
  204.3 1.1 fusion.78
  205.5 1.1 fusion.78
  206.7 1.1 fusion.78
  208.0 1.1 fusion.78
  209.2 0.1 copy.107
  209.3 0.1 multiply_add_fusion.1
  209.7 1.4 fusion.44
  211.1 1.3 fusion.68
  212.5 2.4 %fusion.23 = f32[4,64,2,256]{3,1,0,2:T(8,128)S(1)} fusion(f32[4,64,2]{1,0,2:T(4,128)S(1)} %get-tuple-element.453, bf16[4,64,2,256]{3,2,1,0:T(2,128)(2,1)} %reshape.147, f32[4,2,256,256]{3,2,1,0:T(8,128)S(1)} %copy-done.1, f32[4,2]{1,0:T(4,128)S(1)} %subtract_exponential_fusion.5, f32[2,256,256]{2,1,0:T(8,128)S(1)} %multiply_add_fusion.1, ...), kind=kOutput, calls=%fused_computation.50 | convolution fusion | flops 404357120 | bytes 3409984 | tf_op jit(solution)/shard_map/bhvk,bthk->hbtv/dot_general | solution.py:118
  215.0 0.3 fusion.22
  215.3 0.4 copy.110
  215.7 0.2 copy-done.4
  215.9 0.9 multiply_convert_fusion
  (119 shorter events, 3.0 us)
Async XLA Ops:
  7.2 192.1 %all-gather.7.cloned.1.call-start = ((), (), s32[]{:S(2)}) async-start(), calls=%async_computation | async-start | bytes 2359296 | tf_op jit(solution)/shard_map/all_gather | solution.py:21
  10.8 3.8 %copy-start.2 = (bf16[4,64,2,256]{3,2,1,0:T(2,128)(2,1)}, bf16[4,64,2,256]{3,2,1,0:T(2,128)(2,1)S(1)}, u32[]{:S(2)}) copy-start(bf16[4,64,2,256]{3,2,1,0:T(2,128)(2,1)S(1)} %reshape.148) | copy-start | bytes 786436
  14.5 5.7 %copy-start.6 = (s32[128,2]{0,1:T(2,128)S(1)}, s32[128,2]{0,1:T(2,128)}, u32[]{:S(2)}) copy-start(s32[128,2]{0,1:T(2,128)} %param.29) | copy-start | bytes 3076
  14.5 7.3 %copy-start.9 = (u32[32]{0:T(128)S(1)}, u32[32]{0:T(128)}, u32[]{:S(2)}) copy-start(u32[32]{0:T(128)} %constant.136) | copy-start | bytes 388
  14.5 33.1 %copy-start.3 = (bf16[256,512]{1,0:T(8,128)(2,1)S(1)}, bf16[256,512]{1,0:T(8,128)(2,1)}, u32[]{:S(2)}) copy-start(bf16[256,512]{1,0:T(8,128)(2,1)} %param.19) | copy-start | bytes 786436
  19.3 29.4 %copy-start = (bf16[128,2048]{1,0:T(8,128)(2,1)S(1)}, bf16[128,2048]{1,0:T(8,128)(2,1)}, u32[]{:S(2)}) copy-start(bf16[128,2048]{1,0:T(8,128)(2,1)} %param.27) | copy-start | bytes 1572868
  19.3 29.6 %copy-start.5 = (f32[2048]{0:T(1024)S(1)}, f32[2048]{0:T(1024)}, u32[]{:S(2)}) copy-start(f32[2048]{0:T(1024)} %param.28) | copy-start | bytes 24580
  166.3 2.4 %copy-start.8 = (f32[128,2]{0,1:T(2,128)S(1)}, f32[128,2]{0,1:T(2,128)}, u32[]{:S(2)}) copy-start(f32[128,2]{0,1:T(2,128)} %param.30) | copy-start | bytes 3076
  209.2 3.4 %copy-start.1 = (f32[4,2,256,256]{3,2,1,0:T(8,128)S(1)}, f32[4,2,256,256]{3,2,1,0:T(8,128)}, u32[]{:S(2)}) copy-start(f32[4,2,256,256]{3,2,1,0:T(8,128)} %get-tuple-element.257) | copy-start | bytes 6291460
  214.9 1.0 copy-start.4
  215.0 0.9 copy-start.7
Sparse Core Ops, SparseCore 0:
  20.2 69.8 all-gather.6

commit v2 on v1

--- a/solution.py
+++ b/solution.py
@@ -27,6 +27,14 @@
         return jax.tree.map(lambda a, b: jnp.where(reached, a, b), new, before)
 
     return lax.fori_loop(0, size, step, start)
+
+
+def gathered_carry(device_total):
+    cell, norm, stab, total = device_total
+    zeros = tuple(jnp.zeros_like(part) for part in device_total)
+    identity = zeros[:2] + (jnp.full_like(stab, -1e30),) + zeros[3:]
+    sent_state = (cell.astype(jnp.bfloat16), norm, stab, total)
+    return combine(zeros, carried_in(sent_state, "ep", combine, identity))
 
 
 def combine(earlier, later):
@@ -51,6 +59,7 @@
     forget_gate_logits,
     extra_log_forget,
     cell_output_scale,
+    carry,
 ):
     n_tok, row_width = cell_query_rows.shape
     head_count = row_width // HEAD_DIM
@@ -84,16 +93,8 @@
     def fold_step(running, block_term):
         return (combine(running, block_term), running)
 
-    device_total, before = lax.scan(fold_step, identity_state, block_terms)
-    sent_state = (device_total[0].astype(jnp.bfloat16),) + device_total[1:]
-    prior_state = carried_in(sent_state, "ep", combine, identity_state)
-    zero_state = (
-        jnp.zeros((head_count, HEAD_DIM, HEAD_DIM), jnp.float32),
-        jnp.zeros((head_count, HEAD_DIM), jnp.float32),
-        jnp.zeros((head_count,), jnp.float32),
-        jnp.zeros((head_count,), jnp.float32),
-    )
-    start_state = combine(zero_state, prior_state)
+    device_total, before = lax.scan(fold_step, identity_state, block_terms, unroll=True)
+    start_state = carry(device_total)
     cell_state, norm_state, stabilizer, _ = combine(start_state, before)
     inter_log = cumulative + stabilizer.T[:, :, None]
     causal = jnp.tril(jnp.ones((BLOCK, BLOCK), dtype=bool))
@@ -128,16 +129,16 @@
     ).astype(jnp.bfloat16)
 
 
-def slot_tables(ids, experts, capacity):
-    flat_ids = ids.reshape(-1)
-    onehot = (flat_ids[:, None] == jnp.arange(experts, dtype=jnp.int32)[None, :]).astype(jnp.int32)
-    earlier = jnp.cumsum(onehot, axis=0) - onehot
-    rank_in = jnp.sum(earlier * onehot, axis=1)
-    slot_index = flat_ids * capacity + rank_in
-    token_of = jnp.arange(flat_ids.shape[0], dtype=jnp.int32) // ids.shape[1]
-    slot_hit = slot_index[:, None] == jnp.arange(experts * capacity, dtype=jnp.int32)[None, :]
-    slot_owner = jnp.sum(jnp.where(slot_hit, token_of[:, None] + 1, 0), axis=0)
-    return (slot_owner, slot_index.reshape(ids.shape))
+def slot_masks(ids, experts, capacity):
+    n_tok = ids.shape[0]
+    slots = jnp.arange(experts * capacity, dtype=jnp.int32)[None, :]
+    slot_expert, slot_rank = slots // capacity, slots % capacity
+    chosen = [ids[:, j : j + 1] == slot_expert for j in range(ids.shape[1])]
+    named = functools.reduce(jnp.logical_or, chosen)
+    earlier = jnp.tril(jnp.ones((n_tok, n_tok), jnp.bfloat16), -1)
+    rank = jnp.dot(earlier, named.astype(jnp.bfloat16), preferred_element_type=jnp.float32)
+    hit = jnp.logical_and(named, rank == slot_rank.astype(jnp.float32))
+    return hit, chosen
 
 
 MESH = pl.DeviceIdType.MESH
@@ -146,11 +147,16 @@
 
 def expert_kernel(
     n_ep,
+    heads,
     send_ref,
+    mine_c,
+    mine_aux,
     gate_hbm,
     up_hbm,
     down_hbm,
     ret_ref,
+    in_c,
+    in_aux,
     disp,
     part,
     first,
@@ -161,6 +167,16 @@
     hidden,
     gate_up,
     down,
+    other_c,
+    other_aux,
+    pair_c,
+    pair_aux,
+    next_c,
+    next_aux,
+    chain_c,
+    chain_aux,
+    state_send,
+    state_recv,
     weight_sem,
     local_sem,
     sem_a_send,
@@ -237,6 +253,69 @@
         return remote(final.at[k], ret_ref.at[k], sem_r_send.at[k], sem_r_recv.at[k], ((e + n_ep - k) % n_ep, t))
 
     half = n_ep // 2
+    side, step_at = e % 2, e // 2
+    pair_copies = [
+        remote(mine_c, other_c, state_send.at[0], state_recv.at[0], (e + 1 - 2 * side, t)),
+        remote(mine_aux, other_aux, state_send.at[1], state_recv.at[1], (e + 1 - 2 * side, t)),
+    ]
+    chain_copies = [
+        remote(next_c, chain_c, state_send.at[2], state_recv.at[2], ((e + 2) % n_ep, t)),
+        remote(next_aux, chain_aux, state_send.at[3], state_recv.at[3], ((e + 2) % n_ep, t)),
+    ]
+
+    def matrix(ref, h):
+        size = ref.shape[0] // heads
+        return ref[h * size : (h + 1) * size].astype(jnp.float32)
+
+    def state(c_ref, aux_ref, h):
+        n, m, total = (aux_ref[g * heads + h : g * heads + h + 1] for g in range(3))
+        return matrix(c_ref, h), n, m, total
+
+    def joined(early, late):
+        top = jnp.maximum(late[3] + early[2], late[2])
+        keep, take = jnp.exp(late[3] + early[2] - top), jnp.exp(late[2] - top)
+        return keep * early[0] + take * late[0], keep * early[1] + take * late[1], top, early[3] + late[3]
+
+    def put(c_ref, aux_ref, h, parts):
+        size = c_ref.shape[0] // heads
+        c_ref[h * size : (h + 1) * size] = parts[0].astype(c_ref.dtype)
+        for g in range(3):
+            aux_ref[g * heads + h : g * heads + h + 1] = parts[g + 1]
+
+    def pair_total():
+        for copy in pair_copies:
+            copy.wait_recv()
+        for h in range(heads):
+            mine, other = state(mine_c, mine_aux, h), state(other_c, other_aux, h)
+            early = [jnp.where(side == 0, a, b) for a, b in zip(mine, other)]
+            late = [jnp.where(side == 0, b, a) for a, b in zip(mine, other)]
+            put(pair_c, pair_aux, h, joined(early, late))
+
+    def chain(i):
+        @pl.when(step_at == i)
+        def _():
+            if i:
+                for copy in chain_copies:
+                    copy.wait_recv()
+            for h in range(heads):
+                if i:
+                    before = state(chain_c, chain_aux, h)
+                else:
+                    other = state(other_c, other_aux, h)
+                    before = [jnp.zeros_like(a) for a in other]
+                after_other = joined(before, state(other_c, other_aux, h))
+                put(in_c, in_aux, h, [jnp.where(side == 0, a, b) for a, b in zip(before, after_other)])
+                if i + 1 < half:
+                    put(next_c, next_aux, h, joined(before, state(pair_c, pair_aux, h)))
+            if i + 1 < half:
+                for copy in chain_copies:
+                    copy.start()
+
+    in_aux[...] = jnp.zeros_like(in_aux)
+    next_aux[...] = jnp.zeros_like(next_aux)
+    pair_aux[...] = jnp.zeros_like(pair_aux)
+    for copy in pair_copies:
+        copy.start()
     for k in range(half):
         out_copy(k + half).start()
         if k:
@@ -324,12 +403,23 @@
         results(i)
         for k in (i, i + half):
             sum_to_partner(k).start()
+        if i == 0:
+            pair_total()
+        chain(i)
         if i + 1 < half:
             spread_far(i + 1)
         if i:
             sum_rest(i - 1)
     sum_pairs(half - 1)
     sum_rest(half - 1)
+    for copy in pair_copies:
+        copy.wait_send()
+
+    @pl.when(step_at < half - 1)
+    def _():
+        for copy in chain_copies:
+            copy.wait_send()
+
     for k in range(n_ep):
         if k:
             give_back(k).wait_recv()
@@ -342,7 +432,12 @@
         sum_across(k).wait_send()
 
 
-def experts_by_kernel(sendbuf, gate_matrix, up_matrix, down_matrix, n_ep):
+def experts_by_kernel(sendbuf, state, gate_matrix, up_matrix, down_matrix, n_ep):
+    cell, norm, stab, total = state
+    heads, size = norm.shape
+    spread = lambda part: jnp.broadcast_to(part[:, None], (heads, size))
+    aux = jnp.concatenate([norm, spread(stab), spread(total)], axis=0)
+    aux = jnp.pad(aux, ((0, -aux.shape[0] % 8), (0, 0)))
     rows, width = sendbuf.shape
     cap = rows // n_ep
     units = gate_matrix.shape[1]
@@ -351,11 +446,16 @@
     vmem = pltpu.VMEM
     bf16 = jnp.bfloat16
     dma = pltpu.SemaphoreType.DMA
-    return pl.pallas_call(
-        functools.partial(expert_kernel, n_ep),
-        out_shape=jax.ShapeDtypeStruct(block, bf16),
-        in_specs=[pl.BlockSpec(memory_space=pltpu.VMEM)] + [pl.BlockSpec(memory_space=pl.ANY)] * 3,
-        out_specs=pl.BlockSpec(memory_space=pltpu.VMEM),
+    c_shape = (heads * size, size)
+    returned, in_c, in_aux = pl.pallas_call(
+        functools.partial(expert_kernel, n_ep, heads),
+        out_shape=(
+            jax.ShapeDtypeStruct(block, bf16),
+            jax.ShapeDtypeStruct(c_shape, jnp.float32),
+            jax.ShapeDtypeStruct(aux.shape, jnp.float32),
+        ),
+        in_specs=[pl.BlockSpec(memory_space=pltpu.VMEM)] * 3 + [pl.BlockSpec(memory_space=pl.ANY)] * 3,
+        out_specs=[pl.BlockSpec(memory_space=pltpu.VMEM)] * 3,
         scratch_shapes=[
             vmem((n_ep, 4, cap, width), bf16),
             vmem((n_ep, 4, cap, width), bf16),
@@ -367,6 +467,16 @@
             vmem((tiles, 8 * cap, LANES), bf16),
             vmem((tiles, width, 2 * LANES), bf16),
             vmem((width // out_cols, units, out_cols), bf16),
+            vmem(c_shape, bf16),
+            vmem(aux.shape, jnp.float32),
+            vmem(c_shape, jnp.float32),
+            vmem(aux.shape, jnp.float32),
+            vmem(c_shape, bf16),
+            vmem(aux.shape, jnp.float32),
+            vmem(c_shape, bf16),
+            vmem(aux.shape, jnp.float32),
+            dma((4,)),
+            dma((4,)),
             dma((3 * tiles + width // out_cols,)),
             dma,
         ]
@@ -377,7 +487,21 @@
         cost_estimate=pl.CostEstimate(
             flops=24 * rows * width * units, bytes_accessed=6 * width * units, transcendentals=4 * rows * units
         ),
-    )(sendbuf.reshape(block), gate_matrix, up_matrix, down_matrix).reshape(rows, width)
+    )(
+        sendbuf.reshape(block),
+        cell.astype(bf16).reshape(c_shape),
+        aux,
+        gate_matrix,
+        up_matrix,
+        down_matrix,
+    )
+    prior = (
+        in_c.reshape(heads, size, size),
+        in_aux[:heads],
+        in_aux[heads : 2 * heads, 0],
+        in_aux[2 * heads : 3 * heads, 0],
+    )
+    return returned.reshape(rows, width), prior
 
 
 def local(
@@ -397,16 +521,6 @@
     expert_up_weight,
     expert_down_weight,
 ):
-    gated_head_output = mix_heads(
-        cell_query_rows,
-        cell_key_rows,
-        cell_value_rows,
-        output_gate_logits,
-        log_input_gate,
-        forget_gate_logits,
-        extra_log_forget,
-        cell_output_scale,
-    )
     ep_count = lax.axis_size("ep")
     n_tok = tokens_into_experts.shape[0]
     experts = ep_count * expert_gate_weight.shape[0]
@@ -429,14 +543,35 @@
     )
     if by_kernel:
         token_expert_index = (token_expert_index + ep_count - lax.axis_index("ep")) % ep_count
-    slot_owner, slot_index = slot_tables(token_expert_index, experts, capacity)
-    sendbuf = jnp.where(
-        (slot_owner > 0)[:, None],
-        normed[jnp.maximum(slot_owner - 1, 0)],
-        jnp.zeros((), jnp.bfloat16),
-    )
+    hit, chosen = slot_masks(token_expert_index, experts, capacity)
+    sendbuf = lax.dot_general(
+        hit.astype(jnp.bfloat16), normed, (((0,), (0,)), ((), ())), preferred_element_type=jnp.float32
+    ).astype(jnp.bfloat16)
     if by_kernel:
-        returned = experts_by_kernel(sendbuf, gate_matrix, up_matrix, down_matrix, ep_count)
+        box = []
+
+        def carry(device_total):
+            returned, prior = experts_by_kernel(
+                sendbuf, device_total, gate_matrix, up_matrix, down_matrix, ep_count
+            )
+            box.append(returned)
+            return prior
+
+    else:
+        carry = gathered_carry
+    gated_head_output = mix_heads(
+        cell_query_rows,
+        cell_key_rows,
+        cell_value_rows,
+        output_gate_logits,
+        log_input_gate,
+        forget_gate_logits,
+        extra_log_forget,
+        cell_output_scale,
+        carry,
+    )
+    if by_kernel:
+        (returned,) = box
     else:
         arrived = lax.all_to_all(sendbuf, "ep", split_axis=0, concat_axis=0, tiled=True)
         routed_rows = lax.all_gather(arrived, "tp", axis=0, tiled=True)
@@ -450,9 +585,15 @@
             tiled=True,
         )
         returned = lax.all_to_all(summed, "ep", split_axis=0, concat_axis=0, tiled=True)
-    picked = returned[slot_index]
-    expert_output = jnp.sum(
-        chosen_expert_weight[..., None] * picked.astype(jnp.float32), axis=1
+    slot_weight = sum(
+        jnp.where(jnp.logical_and(hit, named), chosen_expert_weight[:, j : j + 1], 0.0)
+        for j, named in enumerate(chosen)
+    )
+    expert_output = jnp.dot(
+        slot_weight,
+        returned.astype(jnp.float32),
+        precision=lax.Precision.HIGHEST,
+        preferred_element_type=jnp.float32,
     ).astype(jnp.bfloat16)
     return (gated_head_output, expert_output)
 

time: 224 us -> 122 us (0.54)
  blocking collectives: 50.1 us -> 0 us
  other arithmetic: 24.5 us -> 5.51 us
  between operations: 15.1 us -> 0.94 us
  local copies, waits for them, and re-layouts: 17.4 us -> 6.31 us
  Pallas kernels: 109 us -> 100 us
    all_gather x1 -> x0, blocking collectives: 26.3 us -> none  [carried_in(): everything = jax.tree.map(lambda part: lax.all_gather(part, axis), x)]
    unnamed x1 -> x0, blocking collectives: 23.8 us -> none
    select_n x26 -> x1, other arithmetic: 11 us -> 0.01 us  [slot_masks(): slot_expert, slot_rank = (slots // capacity, slots % capacity)]
    pallas_call x1, Pallas kernels: 109 us -> 100 us  [experts_by_kernel(): pl.pallas_call(functools.partial(expert_kernel, n_ep, heads), out_shape=(...]
    gather x2 -> x0, local copies, waits for them, and re-layouts: 7.29 us -> none  [the longest x1 4.85 us: local(): picked = returned[slot_index]]
    reduce_sum x3 -> x0, other arithmetic: 4.17 us -> none  [the longest x1 3.93 us: local(): jnp.sum(chosen_expert_weight[..., None] * picked.astype(jnp.float32), axi...]
    dot_general x0 -> x3, matrix products: none -> 3.83 us  [the longest x1 1.92 us: local(): jnp.dot(slot_weight, returned.astype(jnp.float32), precision=lax.Precisio...]
    dynamic_update_slice x8 -> x0, other arithmetic: 3.43 us -> none  [mix_heads(): device_total, before = lax.scan(fold_step, identity_state, block_terms)]
  transfers between devices with their start and end apart: 1 -> 0, of which waited for: 0 -> 0; matrix products, arithmetic and copies ran while one was open for 9% -> 0% of each run, Pallas kernels for 49% -> 0%
where the time goes in v2:
time: 122 us
  Pallas kernels  100 us (82%)
  matrix products  8.56 us (7%)
  local copies, waits for them, and re-layouts  6.31 us (5%)
  other arithmetic  5.51 us (5%)
    pallas_call x1, Pallas kernels, experts_by_kernel(): pl.pallas_call(functools.partial(expert_kernel, n_ep, heads), out_shape=(...  100 us

profile of v2, /device:TPU:0, one launch (start us, length us, event | category | flops | bytes accessed | tf_op | source)
XLA Modules:
  0.0 121.8 jit_solution(9620569548625236612)
XLA Ops:
  0.6 0.7 fusion.78
  1.4 0.1 reshape.819
  1.4 0.5 reduce_window_sum.13
  1.9 0.2 slice_reduce_fusion
  2.1 0.8 add.391
  2.8 0.2 fusion.100
  3.0 0.3 add_maximum_fusion.1
  3.3 0.1 fusion.73
  3.4 1.0 reshape.818
  4.5 1.0 reshape.821
  5.5 2.0 %fusion.26 = f32[4,2,256,256]{3,2,1,0:T(8,128)S(1)} fusion(bf16[4,64,2,256]{3,2,1,0:T(2,128)(2,1)S(1)} %reshape.821, f32[4,64,2]{1,2,0:T(2,128)S(1)} %copy.33, bf16[4,64,2,256]{3,2,1,0:T(2,128)(2,1)S(1)} %reshape.818), kind=kOutput, calls=%fused_computation.38 | convolution fusion | flops 403177472 | bytes 2623488 | tf_op jit(solution)/shard_map/bshv,bshk->bhvk/dot_general | solution.py:83
  7.5 0.3 multiply_add_fusion
  7.8 0.0 copy-start.6
  7.8 0.0 copy-start
  7.8 0.0 copy-start.4
  7.8 0.4 fusion.25
  8.2 0.1 fusion.80
  8.4 1.6 %fusion.18.mine_c = bf16[512,256]{1,0:T(8,128)(2,1)} fusion(f32[1,2,256,256]{3,2,1,0:T(8,128)S(1)} %get-tuple-element.41, f32[1,2,256,256]{3,2,1,0:T(8,128)S(1)} %get-tuple-element.40, f32[1,2,256,256]{3,2,1,0:T(8,128)S(1)} %get-tuple-element.39, f32[1,2,256,256]{3,2,1,0:T(8,128)S(1)} %get-tuple-element.38, f32[512]{0:T(512)S(1)} %bitcast.163, ...), kind=kLoop, calls=%fused_computation.22 | loop fusion | flops 1572864 | bytes 2375680 | tf_op jit(solution)/shard_map/convert_element_type | solution.py:492
  10.0 0.1 pad.18.clone
  10.0 0.1 pad.19.clone
  10.1 0.1 maximum_maximum_fusion
  10.2 0.6 pad.4.mine_aux
  10.8 0.0 copy-done.6
  10.9 0.3 fusion.12
  11.1 0.0 copy-done
  11.1 0.2 fusion.13
  11.3 0.0 copy-done.4
  11.3 1.6 %convolution_convert_fusion = bf16[320,2048]{1,0:T(8,128)(2,1)} fusion(pred[128,320]{0,1:T(32,128)(4,1)S(1)} %fusion.12, bf16[128,2048]{1,0:T(8,128)(2,1)S(1)} %copy-done, f32[2048]{0:T(1024)S(1)} %copy-done.4, f32[128]{0:T(128)S(1)} %add_rsqrt_fusion), kind=kOutput, calls=%fused_computation | convolution fusion | flops 169476096 | bytes 1884672 | tf_op jit(solution)/shard_map/dot_general | solution.py:547
  13.0 0.0 copy-start.2
  13.0 100.5 %shard_map.158 = (bf16[8,40,2048]{2,1,0:T(8,128)(2,1)}, f32[512,256]{1,0:T(8,128)}, f32[8,256]{1,0:T(8,128)}) custom-call(bf16[8,40,2048]{2,1,0:T(8,128)(2,1)} %bitcast.150, bf16[512,256]{1,0:T(8,128)(2,1)} %fusion.18.mine_c, f32[8,256]{1,0:T(8,128)} %pad.4.mine_aux, bf16[2048,896]{1,0:T(8,128)(2,1)} %bitcast.165, bf16[2048,896]{1,0:T(8,128)(2,1)} %bitcast.166, ...), custom_call_target="tpu_custom_call" | custom-call | flops 14092861440 | bytes 11010048 | tf_op jit(solution)/shard_map/pallas_call | solution.py:450
  113.5 0.0 copy-start.8
  113.5 0.9 slice_reduce_fusion.1
  114.3 0.1 subtract_exponential_fusion.2
  114.4 0.1 copy.38
  114.5 0.1 copy.37
  114.6 0.7 slice.89
  115.3 0.1 multiply_add_fusion.3
  115.4 0.1 fusion.63
  115.5 0.0 copy-done.2
  115.5 0.1 reshape.817
  115.6 0.3 fusion.41
  115.9 0.2 fusion.37
  116.1 0.1 add_maximum_fusion
  116.2 0.3 fusion.101
  116.5 0.1 fusion.67
  116.6 0.0 copy-done.8
  116.6 1.5 %fusion.8 = f32[4,64,2,256]{3,1,0,2:T(8,128)S(1)} fusion(f32[4,64,2]{1,0,2:T(4,128)S(1)} %get-tuple-element.17, bf16[4,64,2,256]{3,2,1,0:T(2,128)(2,1)S(1)} %reshape.817, f32[1,2,256,256]{3,2,1,0:T(8,128)S(1)} %get-tuple-element.33, f32[1,2,256,256]{3,2,1,0:T(8,128)S(1)} %get-tuple-element.34, f32[1,2,256,256]{3,2,1,0:T(8,128)S(1)} %get-tuple-element.35, ...), kind=kOutput, calls=%fused_computation.12 | convolution fusion | flops 405929984 | bytes 2885712 | tf_op jit(solution)/shard_map/bhvk,bthk->hbtv/dot_general | solution.py:119
  118.1 0.0 copy-start.3
  118.1 0.0 copy-start.5
  118.1 0.3 fusion.7
  118.4 0.0 copy-start.7
  118.4 0.0 copy-start.1
  118.4 0.4 copy.43
  118.8 0.2 copy-done.3
  119.0 0.0 copy-done.5
  119.0 0.9 multiply_convert_fusion
  119.9 0.0 copy-done.7
  119.9 0.0 copy-done.1
  119.9 1.9 %convolution_convert_fusion.1 = bf16[128,2048]{1,0:T(8,128)(2,1)} fusion(bf16[320,2048]{1,0:T(8,128)(2,1)S(1)} %bitcast.149, pred[128,320]{0,1:T(32,128)(4,1)S(1)} %fusion.12, f32[128]{0:T(128)S(1)} %get-tuple-element.48, f32[128]{0:T(128)S(1)} %get-tuple-element.47, s32[128]{0:T(128)S(1)} %get-tuple-element.61, s32[128]{0:T(128)S(1)} %get-tuple-element.60, ...), kind=kOutput, calls=%fused_computation.1 | convolution fusion | flops 1007181824 | bytes 1879296 | tf_op jit(solution)/shard_map/dot_general | solution.py:592
  (24 shorter events, 0.2 us)
Async XLA Ops:
  7.8 3.0 %copy-start.6 = (s32[128,2]{0,1:T(2,128)S(1)}, s32[128,2]{0,1:T(2,128)}, u32[]{:S(2)}) copy-start(s32[128,2]{0,1:T(2,128)} %param.25) | copy-start | bytes 3076
  7.8 3.3 %copy-start = (bf16[128,2048]{1,0:T(8,128)(2,1)S(1)}, bf16[128,2048]{1,0:T(8,128)(2,1)}, u32[]{:S(2)}) copy-start(bf16[128,2048]{1,0:T(8,128)(2,1)} %param.23) | copy-start | bytes 1572868
  7.8 3.5 %copy-start.4 = (f32[2048]{0:T(1024)S(1)}, f32[2048]{0:T(1024)}, u32[]{:S(2)}) copy-start(f32[2048]{0:T(1024)} %param.24) | copy-start | bytes 24580
  13.0 102.5 %copy-start.2 = (bf16[256,512]{1,0:T(8,128)(2,1)S(1)}, bf16[256,512]{1,0:T(8,128)(2,1)}, u32[]{:S(2)}) copy-start(bf16[256,512]{1,0:T(8,128)(2,1)} %param.15) | copy-start | bytes 786436
  113.5 3.1 %copy-start.8 = (f32[512,256]{1,0:T(8,128)S(1)}, f32[512,256]{1,0:T(8,128)}, u32[]{:S(2)}) copy-start(f32[512,256]{1,0:T(8,128)} %get-tuple-element.6) | copy-start | bytes 1572868
  118.1 1.0 copy-start.3
  118.1 0.9 copy-start.5
  118.4 1.5 %copy-start.7 = (f32[128,2]{0,1:T(2,128)S(1)}, f32[128,2]{0,1:T(2,128)}, u32[]{:S(2)}) copy-start(f32[128,2]{0,1:T(2,128)} %param.26) | copy-start | bytes 3076
  118.4 1.5 %copy-start.1 = (bf16[8,40,2048]{2,1,0:T(8,128)(2,1)S(1)}, bf16[8,40,2048]{2,1,0:T(8,128)(2,1)}, u32[]{:S(2)}) copy-start(bf16[8,40,2048]{2,1,0:T(8,128)(2,1)} %get-tuple-element.7) | copy-start | bytes 3932164
